TPU v7x, 32 devices: a whole 2x2x4 slice. The times are simulated.
32 devices in a mesh: sp: 8 (over z, y), dp: 4 (over x, core).
Axes of the slice: x: 2, y: 2, z: 4, core: 2. Of those that a mesh axis runs over, the one named last changes fastest.
Arguments:
- queries: bfloat16 [4096, 6144], P(('dp', 'sp')), may hold values from -360 to 360
- latent: bfloat16 [4096, 1024], P(('dp', 'sp')), may hold values from -6 to 6
- rope_key: bfloat16 [4096, 64], P(('dp', 'sp')), may hold values from -6 to 6
- latent_gain: float32 [1024], replicated, may hold values from 0.1 to 1.9
- kv_weight: bfloat16 [1024, 8192], P(None, 'dp'), may hold values from -0.1875 to 0.1875
- gate: bfloat16 [4096, 4096], P(('dp', 'sp')), may hold values from -6 to 6
- out_gain: float32 [4096], replicated, may hold values from 0.1 to 1.9
Outputs:
- attended: bfloat16 [4096, 4096], P(('dp', 'sp'))
All inputs are finite; a program needn't handle non-finite values.
Results may differ from a plain program's by a relative error of at most 0.007.
Values may be sent and summed in bfloat16 or wider, within the bound.
A program may use at most 128 MiB of HBM per device.

v0:
```python
import functools

import jax
import jax.numpy as jnp
import numpy as np
from jax import lax
from jax.experimental import pallas as pl
from jax.experimental.pallas import tpu as pltpu
from jax.sharding import PartitionSpec as P

HEADS = 32
NOPE = 128
ROPE = 64
VDIM = 128
QDIM = NOPE + ROPE
PAIR = 2 * QDIM
KDIM = 256

EPS = 1e-06
THETA = 10000.0
LOG2E = 1.4426950408889634

MESH = pl.DeviceIdType.MESH
DN_T = (((1,), (1,)), ((), ()))


def turn(x, cosine, sine, mask):
    partner = jnp.where(mask, pltpu.roll(x, 96, 1), pltpu.roll(x, 32, 1))
    return x * cosine + partner * sine


def kernel(
    n_s, n_d,
    q_ref, lat_ref, rk_ref, lgain_ref, w_ref, gate_ref, ogain_ref, ta_ref, tb_ref,
    out_ref,
    w_v, gate_v, latb, rkb, qb, kbuf, vbuf, rq, ob, orecv,
    w_sem, gate_sem, lat_send, lat_recv, rk_send, rk_recv, relay_lat, relay_rk,
    q_send, q_recv, o_send, o_recv,
):
    s, d = lax.axis_index("sp"), lax.axis_index("dp")
    rows = lat_ref.shape[0]
    heads = HEADS // n_d
    pairs = heads // 2
    groups = n_s // n_d
    half = n_d // 2
    zh, m = s // n_d, s % n_d
    seq = 2 * ((m % half - m // half + half) % half) + m // half
    home = (d % 2) * half + (d // 2 + d % 2) % half
    core = d % 2
    partner = d + 1 - 2 * core

    def send(src, dst, ssem, rsem, ts, td):
        same = (ts == s) & (td == d)

        @pl.when(jnp.logical_not(same))
        def _():
            pltpu.make_async_remote_copy(
                src, dst, ssem, rsem, device_id={"sp": ts, "dp": td}, device_id_type=MESH
            ).start()

        @pl.when(same)
        def _():
            pltpu.make_async_copy(src, dst, rsem).start()

    def sent(src, dst, ssem, rsem, ts, td):
        same = (ts == s) & (td == d)

        @pl.when(jnp.logical_not(same))
        def _():
            pltpu.make_async_remote_copy(
                src, dst, ssem, rsem, device_id={"sp": ts, "dp": td}, device_id_type=MESH
            ).wait_send()

    def arrived(dst, rsem):
        pltpu.make_async_copy(dst, dst, rsem).wait()

    latent_sends = []
    for k in range(groups):
        for pair in range(n_d // 2):
            i = k * (n_d // 2) + pair
            to = (k * n_d + home, 2 * pair + s % 2)
            latent_sends.append((lat_ref, latb.at[s], lat_send.at[i], lat_recv.at[s], *to))
            latent_sends.append((rk_ref, rkb.at[s], rk_send.at[i], rk_recv.at[s], *to))
    query_sends = [
        (
            q_ref.at[:, pl.ds((t * pairs + p) * PAIR, PAIR)], qb.at[m, p],
            q_send.at[t, p], q_recv.at[m, p], zh * n_d + home, jnp.int32(t),
        )
        for p in range(pairs)
        for t in range(n_d)
    ]
    w_copy = pltpu.make_async_copy(w_ref, w_v, w_sem)
    gate_copy = pltpu.make_async_copy(gate_ref, gate_v, gate_sem)

    for args in latent_sends + query_sends:
        send(*args)
    w_copy.start()
    gate_copy.start()
    w_copy.wait()

    lane = lax.broadcasted_iota(jnp.int32, (rows, 128), 1)
    low = lane < 64
    mask = (lane % 64) < 32
    sign = jnp.where(mask, -1.0, 1.0).astype(jnp.float32)

    def tables(block):
        ca, sa = ta_ref[0], ta_ref[1]
        cb, sb = tb_ref[0, block], tb_ref[1, block]
        return ca * cb - sa * sb, (sa * cb + ca * sb) * sign

    def nearest(i):
        if n_s & (n_s - 1):
            return (s + i) % n_s
        out, bit = 0, 1
        while bit < n_s:
            out = out + bit * ((s // bit + i // bit) % 2)
            bit *= 2
        return out

    def key_step(i, carry):
        slot = nearest(i)
        at = pl.ds(pl.multiple_of(slot * rows, rows), rows)
        arrived(latb.at[slot], lat_recv.at[slot])
        arrived(rkb.at[slot], rk_recv.at[slot])

        @pl.when(slot % 2 == core)
        def _():
            for buf, ssem, rsem in ((latb, relay_lat, lat_recv), (rkb, relay_rk, rk_recv)):
                pltpu.make_async_remote_copy(
                    buf.at[slot], buf.at[slot], ssem.at[slot // 2], rsem.at[slot],
                    device_id={"sp": s, "dp": partner}, device_id_type=MESH,
                ).start()

        wide = latb[slot].astype(jnp.float32)
        scale = lax.rsqrt(jnp.mean(wide * wide, axis=-1, keepdims=True) + EPS)
        normed = (wide * scale * lgain_ref[...]).astype(jnp.bfloat16)
        cosine, sine = tables(slot)
        raw = rkb[slot].astype(jnp.float32).T
        rot = turn(jnp.concatenate([raw, jnp.zeros_like(raw)], axis=1), cosine, sine, mask)
        rot_high = pltpu.roll(rot, 64, 1)
        for h in range(heads):
            both = jnp.dot(
                normed, w_v[:, h * 256 : (h + 1) * 256], preferred_element_type=jnp.float32
            )
            plain = both[:, :NOPE]
            if h % 2 == 0:
                first, second = plain, rot
            else:
                moved = pltpu.roll(plain, 64, 1)
                first = jnp.where(low, 0.0, moved)
                second = jnp.where(low, moved, rot_high)
            kbuf[h, at, :128] = first.astype(jnp.bfloat16)
            kbuf[h, at, 128:] = second.astype(jnp.bfloat16)
            vbuf[h, at, :VDIM] = both[:, NOPE:].astype(jnp.bfloat16)
            vbuf[h, at, VDIM:] = jnp.ones((rows, 128), jnp.bfloat16)
        return carry

    lax.fori_loop(0, n_s, key_step, 0)

    factor = LOG2E * QDIM ** -0.5

    def output_send(j, p):
        return (ob.at[j, p], orecv.at[d, p], o_send.at[j, p], o_recv.at[d, p], zh * n_d + j, seq)

    def query_step(i, carry):
        r, p = (i // pairs + m // 2) % half, i % pairs
        for part in range(2):
            slot = 2 * r + part
            arrived(qb.at[slot, p], q_recv.at[slot, p])
            cosine, sine = tables(zh * n_d + slot)
            cosine_high, sine_high = pltpu.roll(cosine, 64, 1), pltpu.roll(sine, 64, 1)
            here = slice(part * rows, (part + 1) * rows)
            rq[here, :128] = qb[slot, p, :, :128]
            x = qb[slot, p, :, 128:256].astype(jnp.float32)
            rq[here, 128:256] = turn(x, cosine, sine, mask).astype(jnp.bfloat16)
            x = qb[slot, p, :, 256:].astype(jnp.float32)
            rq[here, 256:] = turn(x, cosine_high, sine_high, mask).astype(jnp.bfloat16)
        for odd in range(2):
            h = 2 * p + odd
            scores = lax.dot_general(
                rq[:, odd * 128 : odd * 128 + KDIM], kbuf[h], DN_T, preferred_element_type=jnp.float32
            )
            top = jnp.max(scores, axis=-1, keepdims=True)
            raised = jnp.exp2((scores - top) * factor).astype(jnp.bfloat16)
            total = jnp.dot(raised, vbuf[h], preferred_element_type=jnp.float32)
            result = (total[:, :VDIM] / total[:, VDIM:]).astype(jnp.bfloat16)
            at = slice(odd * VDIM, (odd + 1) * VDIM)
            ob[2 * r, p, :, at] = result[:rows]
            ob[2 * r + 1, p, :, at] = result[rows:]
        send(*output_send(2 * r, p))
        send(*output_send(2 * r + 1, p))
        return carry

    lax.fori_loop(0, half * pairs, query_step, 0)

    gate_copy.wait()
    def gated_piece(t, p):
        c = (t * pairs + p) * 2 * VDIM
        g = gate_v[:, c : c + 2 * VDIM].astype(jnp.float32)
        return slice(c, c + 2 * VDIM), orecv[t, p].astype(jnp.float32) * (g / (1.0 + jnp.exp(-g)))

    square = jnp.zeros((rows, 1), jnp.float32)
    for p in range(pairs):
        for t in range(n_d):
            arrived(orecv.at[t, p], o_recv.at[t, p])
            _, gated = gated_piece(t, p)
            square = square + jnp.sum(gated * gated, axis=-1, keepdims=True)
    scale = lax.rsqrt(square / (HEADS * VDIM) + EPS)
    for t in range(n_d):
        for p in range(pairs):
            cols, gated = gated_piece(t, p)
            out_ref[:, cols] = (gated * scale * ogain_ref[:, cols]).astype(jnp.bfloat16)

    for args in latent_sends + query_sends:
        sent(*args)
    for part in range(n_s // 2):
        slot = 2 * part + core
        for buf, ssem, rsem in ((latb, relay_lat, lat_recv), (rkb, relay_rk, rk_recv)):
            pltpu.make_async_remote_copy(
                buf.at[slot], buf.at[slot], ssem.at[part], rsem.at[slot],
                device_id={"sp": s, "dp": partner}, device_id_type=MESH,
            ).wait_send()

    def output_sent(i, carry):
        sent(*output_send(i // pairs, i % pairs))
        return carry

    lax.fori_loop(0, n_d * pairs, output_sent, 0)


def angle_tables(rows, n_s):
    half = ROPE // 2
    inverse = np.zeros(128)
    inverse[:ROPE] = np.tile(THETA ** (-np.arange(half) / half), 2)
    inner = np.arange(rows)[:, None] * inverse[None, :]
    outer = (np.arange(n_s) * rows)[:, None] * inverse[None, :]
    inner = np.stack([np.cos(inner), np.sin(inner)]).astype(np.float32)
    outer = np.stack([np.cos(outer), np.sin(outer)]).astype(np.float32)
    return jnp.asarray(inner), jnp.asarray(outer[:, :, None, :])


def per_device(n_s, n_d, queries, latent, rope_key, latent_gain, kv_weight, gate, out_gain):
    rows, rank = latent.shape
    heads = HEADS // n_d
    pairs = heads // 2
    seq = rows * n_s
    inner, outer = angle_tables(rows, n_s)
    bf = jnp.bfloat16
    dma = pltpu.SemaphoreType.DMA
    vmem = pl.BlockSpec(memory_space=pltpu.VMEM)
    hbm = pl.BlockSpec(memory_space=pl.ANY)
    pieces = n_s // 2
    return pl.pallas_call(
        functools.partial(kernel, n_s, n_d),
        out_shape=jax.ShapeDtypeStruct(gate.shape, bf),
        in_specs=[hbm, vmem, vmem, vmem, hbm, hbm, vmem, vmem, vmem],
        out_specs=vmem,
        scratch_shapes=[
            pltpu.VMEM(kv_weight.shape, bf),
            pltpu.VMEM(gate.shape, bf),
            pltpu.VMEM((n_s, rows, rank), bf),
            pltpu.VMEM((n_s, ROPE, rows), bf),
            pltpu.VMEM((n_d, pairs, rows, PAIR), bf),
            pltpu.VMEM((heads, seq, KDIM), bf),
            pltpu.VMEM((heads, seq, 2 * VDIM), bf),
            pltpu.VMEM((2 * rows, PAIR), bf),
            pltpu.VMEM((n_d, pairs, rows, 2 * VDIM), bf),
            pltpu.VMEM((n_d, pairs, rows, 2 * VDIM), bf),
            dma, dma,
            dma((pieces,)), dma((n_s,)), dma((pieces,)), dma((n_s,)),
            dma((pieces,)), dma((pieces,)),
            *[dma((n_d, pairs))] * 4,
        ],
        compiler_params=pltpu.CompilerParams(
            has_side_effects=True, vmem_limit_bytes=60 * 1024 * 1024
        ),
        name="latent_attention",
    )(
        queries, latent, rope_key.T, latent_gain[None, :], kv_weight, gate, out_gain[None, :],
        inner, outer,
    )


def solution(mesh):
    return jax.shard_map(
        functools.partial(per_device, mesh.shape["sp"], mesh.shape["dp"]),
        mesh=mesh,
        in_specs=(
            P(("dp", "sp"), None),
            P(("dp", "sp"), None),
            P(("dp", "sp"), None),
            P(),
            P(None, "dp"),
            P(("dp", "sp"), None),
            P(),
        ),
        out_specs=P(("dp", "sp"), None),
        check_vma=False,
    )
```

profile of v0, /device:TPU:12, one launch (start us, length us, event | category | flops | bytes accessed | tf_op | source)
XLA Modules:
  0.0 67.7 jit_solution(16665935661420270580)
XLA Ops:
  0.0 65.4 %latent_attention.1 = bf16[128,4096]{1,0:T(8,128)(2,1)} custom-call(bf16[128,6144]{1,0:T(8,128)(2,1)} %q_ref.1, bf16[128,1024]{1,0:T(8,128)(2,1)} %lat_ref.1, bf16[64,128]{1,0:T(8,128)(2,1)} %bitcast.3, f32[1,1024]{1,0:T(1,128)} %bitcast.5, bf16[1024,2048]{1,0:T(8,128)(2,1)} %w_ref.1, bf16[128,4096]{1,0:T(8,128)(2,1)} %gate_ref.1, f32[1,4096]{1,0:T(1,128)} %bitcast.4, ...), custom_call_target="tpu_custom_call" | custom-call | tf_op jit(solution)/shard_map/latent_attention/pallas_call | solution.py:253
  65.4 2.3 %copy.11 = bf16[128,4096]{1,0:T(8,128)(2,1)} copy(bf16[128,4096]{1,0:T(8,128)(2,1)} %latent_attention.1) | data formatting | bytes 2097152
where the time goes:
time: 67.9 us; the launch traced here: 67.7 us
  Pallas kernels  65.4 us (96%)
  local copies, waits for them, and re-layouts  2.29 us (3%)
    pallas_call x1, Pallas kernels, per_device(): pl.pallas_call(functools.partial(kernel, n_s, n_d), out_shape=jax.ShapeDt...  65.4 us
    unnamed x1, local copies, waits for them, and re-layouts  2.29 us

commit v1 on v0

v1 whole, which is shorter than its diff:
```python
import functools

import jax
import jax.numpy as jnp
import numpy as np
from jax import lax
from jax.experimental import pallas as pl
from jax.experimental.pallas import tpu as pltpu
from jax.sharding import PartitionSpec as P

HEADS = 32
NOPE = 128
ROPE = 64
VDIM = 128
QDIM = NOPE + ROPE
PAIR = 2 * QDIM
KDIM = 256

EPS = 1e-06
THETA = 10000.0
LOG2E = 1.4426950408889634

MESH = pl.DeviceIdType.MESH
DN_T = (((1,), (1,)), ((), ()))


def turn(x, cosine, sine, mask):
    partner = jnp.where(mask, pltpu.roll(x, 96, 1), pltpu.roll(x, 32, 1))
    return x * cosine + partner * sine


def kernel(
    n_s, n_d,
    q_ref, lat_ref, rk_ref, lgain_ref, w_ref, gate_ref, ogain_ref, ta_ref, tb_ref,
    out_ref,
    w_v, gate_v, silu, latz, rkz, latb, rkb, normed, rot, qb, kbuf, vbuf, rq, ob, orecv,
    w_sem, gate_sem, lat_send, lat_mid, rk_send, rk_mid, lat_fwd, rk_fwd, lat_recv, rk_recv,
    relay_lat, relay_rk, q_send, q_recv, o_send, o_recv,
):
    s, d = lax.axis_index("sp"), lax.axis_index("dp")
    rows = lat_ref.shape[0]
    heads = HEADS // n_d
    pairs = heads // 2
    half = n_d // 2
    n_z = n_s // half
    groups = n_z // 2
    x, core = d // 2, d % 2
    z, y = s // half, s % half
    zh, zl = z // 2, z % 2
    m = zl * half + y
    seq = 2 * ((y - zl + half) % half) + zl
    home_y = (x + core) % half
    home = core * half + home_y
    host_y = (x + zl) % half
    lead = core != zl
    partner = d + 1 - 2 * core

    def is_self(ts, td):
        return (ts == s) & (td == d)

    def send(src, dst, ssem, rsem, ts, td):
        same = is_self(ts, td)

        @pl.when(jnp.logical_not(same))
        def _():
            pltpu.make_async_remote_copy(
                src, dst, ssem, rsem, device_id={"sp": ts, "dp": td}, device_id_type=MESH
            ).start()

        @pl.when(same)
        def _():
            pltpu.make_async_copy(src, dst, rsem).start()

    def sent(src, dst, ssem, rsem, ts, td):
        same = is_self(ts, td)

        @pl.when(jnp.logical_not(same))
        def _():
            pltpu.make_async_remote_copy(
                src, dst, ssem, rsem, device_id={"sp": ts, "dp": td}, device_id_type=MESH
            ).wait_send()

    def arrived(dst, rsem):
        pltpu.make_async_copy(dst, dst, rsem).wait()

    w_copy = pltpu.make_async_copy(w_ref, w_v, w_sem)
    gate_copy = pltpu.make_async_copy(gate_ref, gate_v, gate_sem)
    w_copy.start()
    gate_copy.start()

    barrier = pltpu.get_barrier_semaphore()

    def greet(ts, td, when=None):
        there = jnp.logical_not(is_self(ts, td))
        if when is not None:
            there = there & when

        @pl.when(there)
        def _():
            pl.semaphore_signal(
                barrier, inc=1, device_id={"sp": ts, "dp": td}, device_id_type=MESH
            )

    for k in range(n_z):
        greet(k * half + y, 2 * x + zl, lead)
    for k in range(half):
        greet(z * half + k, 2 * (seq // 2) + core, lead)
    greet(s, partner, jnp.logical_not(lead))
    for k in range(n_d):
        greet(zh * n_d + k, seq)
        greet(zh * n_d + home, jnp.int32(k))

    def others(ts, td, count):
        return count - jnp.where(is_self(ts, td), 1, 0)

    meets = groups + others(zh * n_d + home, d, n_d) + others(s, seq, n_d)
    meets = meets + jnp.where(lead, 1 + others(z * half + host_y, d, half), 0)
    pl.semaphore_wait(barrier, meets)

    first_sends = []
    for k in range(groups):
        to = ((2 * k + core) * half + y, partner)
        first_sends.append((lat_ref, latz.at[z], lat_send.at[k], lat_mid.at[z], *to))
        first_sends.append((rk_ref, rkz.at[z], rk_send.at[k], rk_mid.at[z], *to))

    def forwards(from_z):
        slot = from_z * half + y
        for k in range(half):
            to = (z * half + host_y, 2 * k + core)
            yield latz.at[from_z], latb.at[slot], lat_fwd.at[from_z, k], lat_recv.at[slot], *to
            yield rkz.at[from_z], rkb.at[slot], rk_fwd.at[from_z, k], rk_recv.at[slot], *to

    def relays(slot):
        to = {"sp": s, "dp": partner}
        for buf, ssem, rsem in ((latb, relay_lat, lat_recv), (rkb, relay_rk, rk_recv)):
            yield pltpu.make_async_remote_copy(
                buf.at[slot], buf.at[slot], ssem.at[slot], rsem.at[slot],
                device_id=to, device_id_type=MESH,
            )

    query_sends = [
        (
            q_ref.at[:, pl.ds((t * pairs + p) * PAIR, PAIR)], qb.at[m, p],
            q_send.at[t, p], q_recv.at[m, p], zh * n_d + home, jnp.int32(t),
        )
        for p in range(pairs)
        for t in range(n_d)
    ]

    for args in first_sends:
        send(*args)

    @pl.when(jnp.logical_not(lead))
    def _():
        for args in query_sends:
            send(*args)

    gate_copy.wait()
    for c in range(0, HEADS * VDIM, 2 * VDIM):
        at = slice(c, c + 2 * VDIM)
        g = gate_v[:, at].astype(jnp.float32)
        silu[:, at] = g / (1.0 + jnp.exp(-g))

    lane = lax.broadcasted_iota(jnp.int32, (rows, 128), 1)
    mask = (lane % 64) < 32
    sign = jnp.where(mask, -1.0, 1.0).astype(jnp.float32)
    low = lax.broadcasted_iota(jnp.int32, (half * rows, 128), 1) < 64

    def tables(block):
        ca, sa = ta_ref[0], ta_ref[1]
        cb, sb = tb_ref[0, block], tb_ref[1, block]
        return ca * cb - sa * sb, (sa * cb + ca * sb) * sign

    def nearest(here, i, count):
        if count & (count - 1):
            return (here + i) % count
        out, bit = 0, 1
        while bit < count:
            out = out + bit * ((here // bit + i // bit) % 2)
            bit *= 2
        return out

    w_copy.wait()

    def forward_step(i):
        @pl.when(lead)
        def _():
            from_z = nearest(z, i, n_z)
            arrived(latz.at[from_z], lat_mid.at[from_z])
            arrived(rkz.at[from_z], rk_mid.at[from_z])
            for args in forwards(from_z):
                send(*args)

            @pl.when(i == n_z - 1)
            def _():
                for args in query_sends:
                    send(*args)

    def key_step(i, carry):
        @pl.when(i + 1 < n_z)
        def _():
            forward_step(i + 1)

        from_z = nearest(z, i, n_z)
        for k in range(half):
            slot = from_z * half + k
            here = slice(k * rows, (k + 1) * rows)
            arrived(latb.at[slot], lat_recv.at[slot])
            arrived(rkb.at[slot], rk_recv.at[slot])

            @pl.when(lead)
            def _():
                for copy in relays(slot):
                    copy.start()

            wide = latb[slot].astype(jnp.float32)
            scale = lax.rsqrt(jnp.mean(wide * wide, axis=-1, keepdims=True) + EPS)
            normed[here, :] = (wide * scale * lgain_ref[...]).astype(jnp.bfloat16)
            cosine, sine = tables(slot)
            raw = rkb[slot].astype(jnp.float32).T
            rot[here, :] = turn(
                jnp.concatenate([raw, jnp.zeros_like(raw)], axis=1), cosine, sine, mask
            )
        at = pl.ds(pl.multiple_of(from_z * half * rows, half * rows), half * rows)
        for h in range(heads):
            both = jnp.dot(
                normed[...], w_v[:, h * 256 : (h + 1) * 256], preferred_element_type=jnp.float32
            )
            plain = both[:, :NOPE]
            if h % 2 == 0:
                first, second = plain, rot[...]
            else:
                moved = pltpu.roll(plain, 64, 1)
                first = jnp.where(low, 0.0, moved)
                second = jnp.where(low, moved, pltpu.roll(rot[...], 64, 1))
            kbuf[h, at, :128] = first.astype(jnp.bfloat16)
            kbuf[h, at, 128:] = second.astype(jnp.bfloat16)
            vbuf[h, at, :VDIM] = both[:, NOPE:].astype(jnp.bfloat16)
            vbuf[h, at, VDIM:] = jnp.ones((half * rows, 128), jnp.bfloat16)
        return carry

    forward_step(jnp.int32(0))
    lax.fori_loop(0, n_z, key_step, 0)

    factor = LOG2E * QDIM ** -0.5

    def output_send(j, p):
        return (ob.at[j, p], orecv.at[d, p], o_send.at[j, p], o_recv.at[d, p], zh * n_d + j, seq)

    def query_step(i, carry):
        r, p = (i // pairs + m // 2) % half, i % pairs
        for part in range(2):
            slot = 2 * r + part
            arrived(qb.at[slot, p], q_recv.at[slot, p])
            cosine, sine = tables(zh * n_d + slot)
            cosine_high, sine_high = pltpu.roll(cosine, 64, 1), pltpu.roll(sine, 64, 1)
            here = slice(part * rows, (part + 1) * rows)
            rq[here, :128] = qb[slot, p, :, :128]
            v = qb[slot, p, :, 128:256].astype(jnp.float32)
            rq[here, 128:256] = turn(v, cosine, sine, mask).astype(jnp.bfloat16)
            v = qb[slot, p, :, 256:].astype(jnp.float32)
            rq[here, 256:] = turn(v, cosine_high, sine_high, mask).astype(jnp.bfloat16)
        for odd in range(2):
            h = 2 * p + odd
            scores = lax.dot_general(
                rq[:, odd * 128 : odd * 128 + KDIM], kbuf[h], DN_T, preferred_element_type=jnp.float32
            )
            top = jnp.max(scores, axis=-1, keepdims=True)
            raised = jnp.exp2((scores - top) * factor).astype(jnp.bfloat16)
            total = jnp.dot(raised, vbuf[h], preferred_element_type=jnp.float32)
            result = (total[:, :VDIM] / total[:, VDIM:]).astype(jnp.bfloat16)
            at = slice(odd * VDIM, (odd + 1) * VDIM)
            ob[2 * r, p, :, at] = result[:rows]
            ob[2 * r + 1, p, :, at] = result[rows:]
        send(*output_send(2 * r, p))
        send(*output_send(2 * r + 1, p))
        return carry

    lax.fori_loop(0, half * pairs, query_step, 0)

    square = jnp.zeros((rows, 1), jnp.float32)
    for p in range(pairs):
        for t in range(n_d):
            c = (t * pairs + p) * 2 * VDIM
            at = slice(c, c + 2 * VDIM)
            arrived(orecv.at[t, p], o_recv.at[t, p])
            gated = orecv[t, p].astype(jnp.float32) * silu[:, at]
            silu[:, at] = gated
            square = square + jnp.sum(gated * gated, axis=-1, keepdims=True)
    scale = lax.rsqrt(square / (HEADS * VDIM) + EPS)
    for c in range(0, HEADS * VDIM, 2 * VDIM):
        at = slice(c, c + 2 * VDIM)
        out_ref[:, at] = (silu[:, at] * scale * ogain_ref[:, at]).astype(jnp.bfloat16)

    for args in first_sends + query_sends:
        sent(*args)

    @pl.when(lead)
    def _():
        def forwarded(i, carry):
            for args in forwards(i):
                sent(*args)
            for k in range(half):
                for copy in relays(i * half + k):
                    copy.wait_send()
            return carry

        lax.fori_loop(0, n_z, forwarded, 0)

    def output_sent(i, carry):
        sent(*output_send(i // pairs, i % pairs))
        return carry

    lax.fori_loop(0, n_d * pairs, output_sent, 0)


def angle_tables(rows, n_s):
    half = ROPE // 2
    inverse = np.zeros(128)
    inverse[:ROPE] = np.tile(THETA ** (-np.arange(half) / half), 2)
    inner = np.arange(rows)[:, None] * inverse[None, :]
    outer = (np.arange(n_s) * rows)[:, None] * inverse[None, :]
    inner = np.stack([np.cos(inner), np.sin(inner)]).astype(np.float32)
    outer = np.stack([np.cos(outer), np.sin(outer)]).astype(np.float32)
    return jnp.asarray(inner), jnp.asarray(outer[:, :, None, :])


def per_device(n_s, n_d, queries, latent, rope_key, latent_gain, kv_weight, gate, out_gain):
    rows, rank = latent.shape
    heads = HEADS // n_d
    pairs = heads // 2
    seq = rows * n_s
    inner, outer = angle_tables(rows, n_s)
    bf = jnp.bfloat16
    dma = pltpu.SemaphoreType.DMA
    vmem = pl.BlockSpec(memory_space=pltpu.VMEM)
    hbm = pl.BlockSpec(memory_space=pl.ANY)
    half = n_d // 2
    n_z = n_s // half
    return pl.pallas_call(
        functools.partial(kernel, n_s, n_d),
        out_shape=jax.ShapeDtypeStruct(gate.shape, bf),
        in_specs=[hbm, vmem, vmem, vmem, hbm, hbm, vmem, vmem, vmem],
        out_specs=vmem,
        scratch_shapes=[
            pltpu.VMEM(kv_weight.shape, bf),
            pltpu.VMEM(gate.shape, bf),
            pltpu.VMEM(gate.shape, jnp.float32),
            pltpu.VMEM((n_z, rows, rank), bf),
            pltpu.VMEM((n_z, ROPE, rows), bf),
            pltpu.VMEM((n_s, rows, rank), bf),
            pltpu.VMEM((n_s, ROPE, rows), bf),
            pltpu.VMEM((half * rows, rank), bf),
            pltpu.VMEM((half * rows, 128), jnp.float32),
            pltpu.VMEM((n_d, pairs, rows, PAIR), bf),
            pltpu.VMEM((heads, seq, KDIM), bf),
            pltpu.VMEM((heads, seq, 2 * VDIM), bf),
            pltpu.VMEM((2 * rows, PAIR), bf),
            pltpu.VMEM((n_d, pairs, rows, 2 * VDIM), bf),
            pltpu.VMEM((n_d, pairs, rows, 2 * VDIM), bf),
            dma, dma,
            dma((n_z // 2,)), dma((n_z,)), dma((n_z // 2,)), dma((n_z,)),
            dma((n_z, half)), dma((n_z, half)),
            *[dma((n_s,))] * 4,
            *[dma((n_d, pairs))] * 4,
        ],
        compiler_params=pltpu.CompilerParams(
            collective_id=0, has_side_effects=True, vmem_limit_bytes=60 * 1024 * 1024
        ),
        name="latent_attention",
    )(
        queries, latent, rope_key.T, latent_gain[None, :], kv_weight, gate, out_gain[None, :],
        inner, outer,
    )


def solution(mesh):
    return jax.shard_map(
        functools.partial(per_device, mesh.shape["sp"], mesh.shape["dp"]),
        mesh=mesh,
        in_specs=(
            P(("dp", "sp"), None),
            P(("dp", "sp"), None),
            P(("dp", "sp"), None),
            P(),
            P(None, "dp"),
            P(("dp", "sp"), None),
            P(),
        ),
        out_specs=P(("dp", "sp"), None),
        check_vma=False,
    )
```

time: 67.9 us -> 61.7 us (0.909)
  the two profiles are of different devices: /device:TPU:12 before, /device:TPU:1 now
where the time goes in v1:
time: 61.7 us; the launch traced here: 61.6 us
  Pallas kernels  59.3 us (96%)
  local copies, waits for them, and re-layouts  2.29 us (4%)
    pallas_call x1, Pallas kernels, per_device(): pl.pallas_call(functools.partial(kernel, n_s, n_d), out_shape=jax.ShapeDt...  59.3 us
    unnamed x1, local copies, waits for them, and re-layouts  2.29 us

profile of v1, /device:TPU:1, one launch (start us, length us, event | category | flops | bytes accessed | tf_op | source)
XLA Modules:
  0.0 61.6 jit_solution(15313377206373783618)
XLA Ops:
  0.0 59.3 %latent_attention.1 = bf16[128,4096]{1,0:T(8,128)(2,1)} custom-call(bf16[128,6144]{1,0:T(8,128)(2,1)} %q_ref.1, bf16[128,1024]{1,0:T(8,128)(2,1)} %lat_ref.1, bf16[64,128]{1,0:T(8,128)(2,1)} %bitcast.3, f32[1,1024]{1,0:T(1,128)} %bitcast.5, bf16[1024,2048]{1,0:T(8,128)(2,1)} %w_ref.1, bf16[128,4096]{1,0:T(8,128)(2,1)} %gate_ref.1, f32[1,4096]{1,0:T(1,128)} %bitcast.4, ...), custom_call_target="tpu_custom_call" | custom-call | tf_op jit(solution)/shard_map/latent_attention/pallas_call | solution.py:340
  59.3 2.3 %copy.11 = bf16[128,4096]{1,0:T(8,128)(2,1)} copy(bf16[128,4096]{1,0:T(8,128)(2,1)} %latent_attention.1) | data formatting | bytes 2097152

commit v2 on v1

--- a/solution.py
+++ b/solution.py
@@ -19,6 +19,8 @@
 EPS = 1e-06
 THETA = 10000.0
 LOG2E = 1.4426950408889634
+CHUNKS = 2
+QUERIES_AT = (0, 2, 5, 8)
 
 MESH = pl.DeviceIdType.MESH
 DN_T = (((1,), (1,)), ((), ()))
@@ -31,10 +33,10 @@
 
 def kernel(
     n_s, n_d,
-    q_ref, lat_ref, rk_ref, lgain_ref, w_ref, gate_ref, ogain_ref, ta_ref, tb_ref,
-    out_ref,
-    w_v, gate_v, silu, latz, rkz, latb, rkb, normed, rot, qb, kbuf, vbuf, rq, ob, orecv,
-    w_sem, gate_sem, lat_send, lat_mid, rk_send, rk_mid, lat_fwd, rk_fwd, lat_recv, rk_recv,
+    q_ref, lat_ref, rk_ref, lgain_hbm, w_ref, gate_ref, ta_hbm, tb_hbm,
+    gated_ref, scale_ref,
+    w_v, gate_v, lgain_ref, ta_ref, tb_ref, latz, rkz, latb, rkb, normed, rot, qb, kbuf, vbuf, rq, ob, orecv,
+    w_sem, gate_sem, small_sem, lat_send, lat_mid, rk_send, rk_mid, lat_fwd, rk_fwd, lat_recv, rk_recv,
     relay_lat, relay_rk, q_send, q_recv, o_send, o_recv,
 ):
     s, d = lax.axis_index("sp"), lax.axis_index("dp")
@@ -52,11 +54,17 @@
     home_y = (x + core) % half
     home = core * half + home_y
     host_y = (x + zl) % half
-    lead = core != zl
+    lead = core == zl
     partner = d + 1 - 2 * core
+    chunk = rows // CHUNKS
 
     def is_self(ts, td):
         return (ts == s) & (td == d)
+
+    def away(src, dst, ssem, rsem, ts, td):
+        return pltpu.make_async_remote_copy(
+            src, dst, ssem, rsem, device_id={"sp": ts, "dp": td}, device_id_type=MESH
+        )
 
     def send(src, dst, ssem, rsem, ts, td):
         same = is_self(ts, td)
@@ -85,8 +93,16 @@
 
     w_copy = pltpu.make_async_copy(w_ref, w_v, w_sem)
     gate_copy = pltpu.make_async_copy(gate_ref, gate_v, gate_sem)
+    small_copies = [
+        pltpu.make_async_copy(src, dst, small_sem.at[i])
+        for i, (src, dst) in enumerate(
+            ((lgain_hbm, lgain_ref), (ta_hbm, ta_ref), (tb_hbm, tb_ref))
+        )
+    ]
+    gate_copy.start()
     w_copy.start()
-    gate_copy.start()
+    for copy in small_copies:
+        copy.start()
 
     barrier = pltpu.get_barrier_semaphore()
 
@@ -102,10 +118,10 @@
             )
 
     for k in range(n_z):
-        greet(k * half + y, 2 * x + zl, lead)
+        greet(k * half + y, d, lead)
     for k in range(half):
-        greet(z * half + k, 2 * (seq // 2) + core, lead)
-    greet(s, partner, jnp.logical_not(lead))
+        greet(z * half + k, 2 * (seq // 2) + 1 - core, jnp.logical_not(lead))
+    greet(s, partner, lead)
     for k in range(n_d):
         greet(zh * n_d + k, seq)
         greet(zh * n_d + home, jnp.int32(k))
@@ -114,21 +130,36 @@
         return count - jnp.where(is_self(ts, td), 1, 0)
 
     meets = groups + others(zh * n_d + home, d, n_d) + others(s, seq, n_d)
-    meets = meets + jnp.where(lead, 1 + others(z * half + host_y, d, half), 0)
+    meets = meets + jnp.where(lead, half - 1, 1)
+    gate_copy.wait()
+    for c in range(0, HEADS * VDIM, 2 * VDIM):
+        at = slice(c, c + 2 * VDIM)
+        g = gate_v[:, at].astype(jnp.float32)
+        gated_ref[:, at] = g / (1.0 + jnp.exp(-g))
     pl.semaphore_wait(barrier, meets)
 
     first_sends = []
-    for k in range(groups):
-        to = ((2 * k + core) * half + y, partner)
-        first_sends.append((lat_ref, latz.at[z], lat_send.at[k], lat_mid.at[z], *to))
-        first_sends.append((rk_ref, rkz.at[z], rk_send.at[k], rk_mid.at[z], *to))
-
-    def forwards(from_z):
+    for ch in range(CHUNKS):
+        at = pl.ds(ch * chunk, chunk)
+        for k in range(groups):
+            to = ((2 * k + core) * half + y, d)
+            first_sends.append(
+                (lat_ref.at[at], latz.at[z, at], lat_send.at[k, ch], lat_mid.at[z, ch], *to)
+            )
+            if ch == 0:
+                first_sends.append((rk_ref, rkz.at[z], rk_send.at[k], rk_mid.at[z], *to))
+
+    def forwards(from_z, ch):
         slot = from_z * half + y
+        at = pl.ds(ch * chunk, chunk)
         for k in range(half):
-            to = (z * half + host_y, 2 * k + core)
-            yield latz.at[from_z], latb.at[slot], lat_fwd.at[from_z, k], lat_recv.at[slot], *to
-            yield rkz.at[from_z], rkb.at[slot], rk_fwd.at[from_z, k], rk_recv.at[slot], *to
+            to = (z * half + host_y, 2 * k + 1 - zl)
+            yield (
+                latz.at[from_z, at], latb.at[slot, at], lat_fwd.at[from_z, k, ch],
+                lat_recv.at[slot], *to,
+            )
+            if ch == 0:
+                yield rkz.at[from_z], rkb.at[slot], rk_fwd.at[from_z, k], rk_recv.at[slot], *to
 
     def relays(slot):
         to = {"sp": s, "dp": partner}
@@ -150,16 +181,14 @@
     for args in first_sends:
         send(*args)
 
+    def query_part(p):
+        for args in query_sends[p * n_d : (p + 1) * n_d]:
+            send(*args)
+
     @pl.when(jnp.logical_not(lead))
     def _():
-        for args in query_sends:
-            send(*args)
-
-    gate_copy.wait()
-    for c in range(0, HEADS * VDIM, 2 * VDIM):
-        at = slice(c, c + 2 * VDIM)
-        g = gate_v[:, at].astype(jnp.float32)
-        silu[:, at] = g / (1.0 + jnp.exp(-g))
+        for p in range(pairs):
+            query_part(p)
 
     lane = lax.broadcasted_iota(jnp.int32, (rows, 128), 1)
     mask = (lane % 64) < 32
@@ -181,26 +210,29 @@
         return out
 
     w_copy.wait()
-
-    def forward_step(i):
-        @pl.when(lead)
-        def _():
+    for copy in small_copies:
+        copy.wait()
+
+    @pl.when(lead)
+    def _():
+        order = [(0, ch) for ch in range(CHUNKS)]
+        order += [(i, ch) for ch in range(CHUNKS) for i in range(1, n_z)]
+        for n, (i, ch) in enumerate(order):
+            for p in range(pairs):
+                if QUERIES_AT[p] == n:
+                    query_part(p)
             from_z = nearest(z, i, n_z)
-            arrived(latz.at[from_z], lat_mid.at[from_z])
-            arrived(rkz.at[from_z], rk_mid.at[from_z])
-            for args in forwards(from_z):
-                send(*args)
-
-            @pl.when(i == n_z - 1)
-            def _():
-                for args in query_sends:
-                    send(*args)
+            at = pl.ds(ch * chunk, chunk)
+            arrived(latz.at[from_z, at], lat_mid.at[from_z, ch])
+            if ch == 0:
+                arrived(rkz.at[from_z], rk_mid.at[from_z])
+            for args in forwards(from_z, ch):
+                away(*args).start()
+        for p in range(pairs):
+            if QUERIES_AT[p] >= len(order):
+                query_part(p)
 
     def key_step(i, carry):
-        @pl.when(i + 1 < n_z)
-        def _():
-            forward_step(i + 1)
-
         from_z = nearest(z, i, n_z)
         for k in range(half):
             slot = from_z * half + k
@@ -208,7 +240,7 @@
             arrived(latb.at[slot], lat_recv.at[slot])
             arrived(rkb.at[slot], rk_recv.at[slot])
 
-            @pl.when(lead)
+            @pl.when(jnp.logical_not(lead))
             def _():
                 for copy in relays(slot):
                     copy.start()
@@ -239,7 +271,6 @@
             vbuf[h, at, VDIM:] = jnp.ones((half * rows, 128), jnp.bfloat16)
         return carry
 
-    forward_step(jnp.int32(0))
     lax.fori_loop(0, n_z, key_step, 0)
 
     factor = LOG2E * QDIM ** -0.5
@@ -248,7 +279,7 @@
         return (ob.at[j, p], orecv.at[d, p], o_send.at[j, p], o_recv.at[d, p], zh * n_d + j, seq)
 
     def query_step(i, carry):
-        r, p = (i // pairs + m // 2) % half, i % pairs
+        r, p = (i % half + m // 2) % half, i // half
         for part in range(2):
             slot = 2 * r + part
             arrived(qb.at[slot, p], q_recv.at[slot, p])
@@ -284,28 +315,30 @@
             c = (t * pairs + p) * 2 * VDIM
             at = slice(c, c + 2 * VDIM)
             arrived(orecv.at[t, p], o_recv.at[t, p])
-            gated = orecv[t, p].astype(jnp.float32) * silu[:, at]
-            silu[:, at] = gated
+            gated = orecv[t, p].astype(jnp.float32) * gated_ref[:, at]
+            gated_ref[:, at] = gated
             square = square + jnp.sum(gated * gated, axis=-1, keepdims=True)
     scale = lax.rsqrt(square / (HEADS * VDIM) + EPS)
-    for c in range(0, HEADS * VDIM, 2 * VDIM):
-        at = slice(c, c + 2 * VDIM)
-        out_ref[:, at] = (silu[:, at] * scale * ogain_ref[:, at]).astype(jnp.bfloat16)
+    scale_ref[...] = jnp.broadcast_to(scale, scale_ref.shape)
 
     for args in first_sends + query_sends:
         sent(*args)
 
     @pl.when(lead)
     def _():
-        def forwarded(i, carry):
-            for args in forwards(i):
-                sent(*args)
-            for k in range(half):
-                for copy in relays(i * half + k):
-                    copy.wait_send()
+        for i in range(n_z):
+            for ch in range(CHUNKS):
+                for args in forwards(i, ch):
+                    away(*args).wait_send()
+
+    @pl.when(jnp.logical_not(lead))
+    def _():
+        def relayed(i, carry):
+            for copy in relays(i):
+                copy.wait_send()
             return carry
 
-        lax.fori_loop(0, n_z, forwarded, 0)
+        lax.fori_loop(0, n_s, relayed, 0)
 
     def output_sent(i, carry):
         sent(*output_send(i // pairs, i % pairs))
@@ -337,15 +370,20 @@
     hbm = pl.BlockSpec(memory_space=pl.ANY)
     half = n_d // 2
     n_z = n_s // half
-    return pl.pallas_call(
+    gated, scale = pl.pallas_call(
         functools.partial(kernel, n_s, n_d),
-        out_shape=jax.ShapeDtypeStruct(gate.shape, bf),
-        in_specs=[hbm, vmem, vmem, vmem, hbm, hbm, vmem, vmem, vmem],
-        out_specs=vmem,
+        out_shape=(
+            pltpu.VMEM(gate.shape, jnp.float32),
+            pltpu.VMEM((rows, 128), jnp.float32),
+        ),
+        in_specs=[hbm] * 8,
+        out_specs=(vmem, vmem),
         scratch_shapes=[
             pltpu.VMEM(kv_weight.shape, bf),
             pltpu.VMEM(gate.shape, bf),
-            pltpu.VMEM(gate.shape, jnp.float32),
+            pltpu.VMEM((1, rank), jnp.float32),
+            pltpu.VMEM(inner.shape, jnp.float32),
+            pltpu.VMEM(outer.shape, jnp.float32),
             pltpu.VMEM((n_z, rows, rank), bf),
             pltpu.VMEM((n_z, ROPE, rows), bf),
             pltpu.VMEM((n_s, rows, rank), bf),
@@ -358,9 +396,9 @@
             pltpu.VMEM((2 * rows, PAIR), bf),
             pltpu.VMEM((n_d, pairs, rows, 2 * VDIM), bf),
             pltpu.VMEM((n_d, pairs, rows, 2 * VDIM), bf),
-            dma, dma,
-            dma((n_z // 2,)), dma((n_z,)), dma((n_z // 2,)), dma((n_z,)),
-            dma((n_z, half)), dma((n_z, half)),
+            dma, dma, dma((3,)),
+            dma((n_z // 2, CHUNKS)), dma((n_z, CHUNKS)), dma((n_z // 2,)), dma((n_z,)),
+            dma((n_z, half, CHUNKS)), dma((n_z, half)),
             *[dma((n_s,))] * 4,
             *[dma((n_d, pairs))] * 4,
         ],
@@ -369,9 +407,9 @@
         ),
         name="latent_attention",
     )(
-        queries, latent, rope_key.T, latent_gain[None, :], kv_weight, gate, out_gain[None, :],
-        inner, outer,
+        queries, latent, rope_key.T, latent_gain[None, :], kv_weight, gate, inner, outer,
     )
+    return (gated * scale[:, :1] * out_gain[None, :]).astype(bf)
 
 
 def solution(mesh):

time: 61.7 us -> 56.7 us (0.919)
  Pallas kernels: 59.3 us -> 54.7 us
  local copies, waits for them, and re-layouts: 2.29 us -> 0.11 us
  other arithmetic: 0 us -> 1.25 us
    pallas_call x1, Pallas kernels: 59.3 us -> 54.7 us  [per_device(): pl.pallas_call(functools.partial(kernel, n_s, n_d), out_shape=(pltpu.VMEM...]
    unnamed x1 -> x2, local copies, waits for them, and re-layouts: 2.29 us -> 0.01 us
    convert_element_type x0 -> x1, other arithmetic: none -> 1.25 us  [per_device(): return (gated * scale[:, :1] * out_gain[None, :]).astype(bf)]
where the time goes in v2:
time: 56.7 us; the launch traced here: 56.1 us
  Pallas kernels  54.7 us (96%)
  other arithmetic  1.25 us (2%)
    pallas_call x1, Pallas kernels, per_device(): pl.pallas_call(functools.partial(kernel, n_s, n_d), out_shape=(pltpu.VMEM...  54.7 us
    convert_element_type x1, other arithmetic, per_device(): return (gated * scale[:, :1] * out_gain[None, :]).astype(bf)  1.25 us

profile of v2, /device:TPU:1, one launch (start us, length us, event | category | flops | bytes accessed | tf_op | source)
XLA Modules:
  0.0 56.1 jit_solution(10513523949264622149)
XLA Ops:
  0.0 0.0 copy-start
  0.0 54.7 %latent_attention.1 = (f32[128,4096]{1,0:T(8,128)S(1)}, f32[128,128]{1,0:T(8,128)S(1)}) custom-call(bf16[128,6144]{1,0:T(8,128)(2,1)} %q_ref.1, bf16[128,1024]{1,0:T(8,128)(2,1)} %lat_ref.1, bf16[64,128]{1,0:T(8,128)(2,1)} %bitcast.2, f32[1,1024]{1,0:T(1,128)} %bitcast.3, bf16[1024,2048]{1,0:T(8,128)(2,1)} %w_ref.1, bf16[128,4096]{1,0:T(8,128)(2,1)} %gate_ref.1, ...), custom_call_target="tpu_custom_call" | custom-call | tf_op jit(solution)/shard_map/latent_attention/pallas_call | solution.py:373
  54.7 0.1 slice_reduce_fusion
  54.8 0.0 copy-done
  54.8 1.3 %multiply_convert_fusion = bf16[128,4096]{1,0:T(8,128)(2,1)} fusion(f32[128,4096]{1,0:T(8,128)S(1)} %get-tuple-element.7, f32[4096]{0:T(1024)S(1)} %copy-done, f32[128]{0:T(128)S(1)} %slice_reduce_fusion), kind=kLoop, calls=%fused_computation | loop fusion | flops 1572864 | bytes 3162624 | tf_op jit(solution)/shard_map/convert_element_type | solution.py:412
Async XLA Ops:
  0.0 54.8 %copy-start = (f32[4096]{0:T(1024)S(1)}, f32[4096]{0:T(1024)}, u32[]{:S(2)}) copy-start(f32[4096]{0:T(1024)} %param.15) | copy-start | bytes 49156

commit v3 on v2

--- a/solution.py
+++ b/solution.py
@@ -20,7 +20,9 @@
 THETA = 10000.0
 LOG2E = 1.4426950408889634
 CHUNKS = 2
-QUERIES_AT = (0, 2, 5, 8)
+QUERIES_AT = (0, 2, 4, 8)
+CROSSING_AT = (0, 1, 2, 3)
+TARGETS = (0, 1, 2, 3)
 
 MESH = pl.DeviceIdType.MESH
 DN_T = (((1,), (1,)), ((), ()))
@@ -169,14 +171,15 @@
                 device_id=to, device_id_type=MESH,
             )
 
-    query_sends = [
-        (
-            q_ref.at[:, pl.ds((t * pairs + p) * PAIR, PAIR)], qb.at[m, p],
-            q_send.at[t, p], q_recv.at[m, p], zh * n_d + home, jnp.int32(t),
-        )
-        for p in range(pairs)
-        for t in range(n_d)
-    ]
+    def query_sends_of(p):
+        for t in TARGETS:
+            t = ((x + t // 2) % half) * 2 + (core + t % 2) % 2
+            yield (
+                q_ref.at[:, pl.ds(pl.multiple_of((t * pairs + p) * PAIR, PAIR), PAIR)],
+                qb.at[m, p], q_send.at[t, p], q_recv.at[m, p], zh * n_d + home, t,
+            )
+
+    query_sends = [args for p in range(pairs) for args in query_sends_of(p)]
 
     for args in first_sends:
         send(*args)
@@ -188,7 +191,8 @@
     @pl.when(jnp.logical_not(lead))
     def _():
         for p in range(pairs):
-            query_part(p)
+            if CROSSING_AT[p % len(CROSSING_AT)] == 0:
+                query_part(p)
 
     lane = lax.broadcasted_iota(jnp.int32, (rows, 128), 1)
     mask = (lane % 64) < 32
@@ -213,13 +217,14 @@
     for copy in small_copies:
         copy.wait()
 
-    @pl.when(lead)
-    def _():
-        order = [(0, ch) for ch in range(CHUNKS)]
-        order += [(i, ch) for ch in range(CHUNKS) for i in range(1, n_z)]
-        for n, (i, ch) in enumerate(order):
+    stages = [[(i, ch) for i in range(2) for ch in range(CHUNKS)]]
+    stages += [[(i, ch) for i in range(2, n_z)] for ch in range(CHUNKS)]
+    starts = [sum(map(len, stages[:k])) for k in range(len(stages) + 1)]
+
+    def forward_stage(k):
+        for n, (i, ch) in enumerate(stages[k], starts[k]):
             for p in range(pairs):
-                if QUERIES_AT[p] == n:
+                if QUERIES_AT[p % len(QUERIES_AT)] == n:
                     query_part(p)
             from_z = nearest(z, i, n_z)
             at = pl.ds(ch * chunk, chunk)
@@ -228,11 +233,18 @@
                 arrived(rkz.at[from_z], rk_mid.at[from_z])
             for args in forwards(from_z, ch):
                 away(*args).start()
-        for p in range(pairs):
-            if QUERIES_AT[p] >= len(order):
-                query_part(p)
+        if k == len(stages) - 1:
+            for p in range(pairs):
+                if QUERIES_AT[p % len(QUERIES_AT)] >= starts[-1]:
+                    query_part(p)
 
     def key_step(i, carry):
+        for k in range(len(stages)):
+
+            @pl.when(lead & (i == k))
+            def _():
+                forward_stage(k)
+
         from_z = nearest(z, i, n_z)
         for k in range(half):
             slot = from_z * half + k
@@ -269,6 +281,13 @@
             kbuf[h, at, 128:] = second.astype(jnp.bfloat16)
             vbuf[h, at, :VDIM] = both[:, NOPE:].astype(jnp.bfloat16)
             vbuf[h, at, VDIM:] = jnp.ones((half * rows, 128), jnp.bfloat16)
+        for step in sorted(set(CROSSING_AT) - {0}):
+
+            @pl.when(jnp.logical_not(lead) & (i + 1 == step))
+            def _():
+                for p in range(pairs):
+                    if CROSSING_AT[p % len(CROSSING_AT)] == step:
+                        query_part(p)
         return carry
 
     lax.fori_loop(0, n_z, key_step, 0)

time: 56.7 us -> 54.5 us (0.961)
  Pallas kernels: 54.7 us -> 53 us
    pallas_call x1, Pallas kernels: 54.7 us -> 53 us  [per_device(): pl.pallas_call(functools.partial(kernel, n_s, n_d), out_shape=(pltpu.VMEM...]
where the time goes in v3:
time: 54.5 us; the launch traced here: 54.4 us
  Pallas kernels  53 us (97%)
  other arithmetic  1.25 us (2%)
    pallas_call x1, Pallas kernels, per_device(): pl.pallas_call(functools.partial(kernel, n_s, n_d), out_shape=(pltpu.VMEM...  53 us
    convert_element_type x1, other arithmetic, per_device(): return (gated * scale[:, :1] * out_gain[None, :]).astype(bf)  1.25 us

profile of v3, /device:TPU:1, one launch (start us, length us, event | category | flops | bytes accessed | tf_op | source)
XLA Modules:
  0.0 54.4 jit_solution(4621786015550189177)
XLA Ops:
  0.0 0.0 copy-start
  0.0 53.0 %latent_attention.1 = (f32[128,4096]{1,0:T(8,128)S(1)}, f32[128,128]{1,0:T(8,128)S(1)}) custom-call(bf16[128,6144]{1,0:T(8,128)(2,1)} %q_ref.1, bf16[128,1024]{1,0:T(8,128)(2,1)} %lat_ref.1, bf16[64,128]{1,0:T(8,128)(2,1)} %bitcast.2, f32[1,1024]{1,0:T(1,128)} %bitcast.3, bf16[1024,2048]{1,0:T(8,128)(2,1)} %w_ref.1, bf16[128,4096]{1,0:T(8,128)(2,1)} %gate_ref.1, ...), custom_call_target="tpu_custom_call" | custom-call | tf_op jit(solution)/shard_map/latent_attention/pallas_call | solution.py:392
  53.0 0.1 slice_reduce_fusion
  53.1 0.0 copy-done
  53.1 1.3 %multiply_convert_fusion = bf16[128,4096]{1,0:T(8,128)(2,1)} fusion(f32[128,4096]{1,0:T(8,128)S(1)} %get-tuple-element.7, f32[4096]{0:T(1024)S(1)} %copy-done, f32[128]{0:T(128)S(1)} %slice_reduce_fusion), kind=kLoop, calls=%fused_computation | loop fusion | flops 1572864 | bytes 3162624 | tf_op jit(solution)/shard_map/convert_element_type | solution.py:431
Async XLA Ops:
  0.0 53.1 %copy-start = (f32[4096]{0:T(1024)S(1)}, f32[4096]{0:T(1024)}, u32[]{:S(2)}) copy-start(f32[4096]{0:T(1024)} %param.15) | copy-start | bytes 49156

commit v4 on v3

--- a/solution.py
+++ b/solution.py
@@ -21,7 +21,7 @@
 LOG2E = 1.4426950408889634
 CHUNKS = 2
 QUERIES_AT = (0, 2, 4, 8)
-CROSSING_AT = (0, 1, 2, 3)
+CROSSING_AT = (0, 0, 2, 3)
 TARGETS = (0, 1, 2, 3)
 
 MESH = pl.DeviceIdType.MESH
@@ -35,9 +35,9 @@
 
 def kernel(
     n_s, n_d,
-    q_ref, lat_ref, rk_ref, lgain_hbm, w_ref, gate_ref, ta_hbm, tb_hbm,
+    q_ref, lat_hbm, rk_hbm, lgain_hbm, w_ref, gate_ref, ta_hbm, tb_hbm,
     gated_ref, scale_ref,
-    w_v, gate_v, lgain_ref, ta_ref, tb_ref, latz, rkz, latb, rkb, normed, rot, qb, kbuf, vbuf, rq, ob, orecv,
+    w_v, gate_v, lat_ref, rk_ref, lgain_ref, ta_ref, tb_ref, latz, rkz, latb, rkb, normed, rot, qb, kbuf, vbuf, rq, ob, orecv,
     w_sem, gate_sem, small_sem, lat_send, lat_mid, rk_send, rk_mid, lat_fwd, rk_fwd, lat_recv, rk_recv,
     relay_lat, relay_rk, q_send, q_recv, o_send, o_recv,
 ):
@@ -98,13 +98,16 @@
     small_copies = [
         pltpu.make_async_copy(src, dst, small_sem.at[i])
         for i, (src, dst) in enumerate(
-            ((lgain_hbm, lgain_ref), (ta_hbm, ta_ref), (tb_hbm, tb_ref))
+            (
+                (lat_hbm, lat_ref), (rk_hbm, rk_ref), (lgain_hbm, lgain_ref),
+                (ta_hbm, ta_ref), (tb_hbm, tb_ref),
+            )
         )
     ]
     gate_copy.start()
-    w_copy.start()
     for copy in small_copies:
         copy.start()
+    w_copy.start()
 
     barrier = pltpu.get_barrier_semaphore()
 
@@ -181,6 +184,8 @@
 
     query_sends = [args for p in range(pairs) for args in query_sends_of(p)]
 
+    for copy in small_copies[:2]:
+        copy.wait()
     for args in first_sends:
         send(*args)
 
@@ -214,7 +219,7 @@
         return out
 
     w_copy.wait()
-    for copy in small_copies:
+    for copy in small_copies[2:]:
         copy.wait()
 
     stages = [[(i, ch) for i in range(2) for ch in range(CHUNKS)]]
@@ -297,14 +302,12 @@
     def output_send(j, p):
         return (ob.at[j, p], orecv.at[d, p], o_send.at[j, p], o_recv.at[d, p], zh * n_d + j, seq)
 
-    def query_step(i, carry):
-        r, p = (i % half + m // 2) % half, i // half
-        for part in range(2):
-            slot = 2 * r + part
+    def query_step(p, carry):
+        for slot in range(n_d):
             arrived(qb.at[slot, p], q_recv.at[slot, p])
             cosine, sine = tables(zh * n_d + slot)
             cosine_high, sine_high = pltpu.roll(cosine, 64, 1), pltpu.roll(sine, 64, 1)
-            here = slice(part * rows, (part + 1) * rows)
+            here = slice(slot * rows, (slot + 1) * rows)
             rq[here, :128] = qb[slot, p, :, :128]
             v = qb[slot, p, :, 128:256].astype(jnp.float32)
             rq[here, 128:256] = turn(v, cosine, sine, mask).astype(jnp.bfloat16)
@@ -320,13 +323,13 @@
             total = jnp.dot(raised, vbuf[h], preferred_element_type=jnp.float32)
             result = (total[:, :VDIM] / total[:, VDIM:]).astype(jnp.bfloat16)
             at = slice(odd * VDIM, (odd + 1) * VDIM)
-            ob[2 * r, p, :, at] = result[:rows]
-            ob[2 * r + 1, p, :, at] = result[rows:]
-        send(*output_send(2 * r, p))
-        send(*output_send(2 * r + 1, p))
+            for slot in range(n_d):
+                ob[slot, p, :, at] = result[slot * rows : (slot + 1) * rows]
+        for slot in range(n_d):
+            send(*output_send(slot, p))
         return carry
 
-    lax.fori_loop(0, half * pairs, query_step, 0)
+    lax.fori_loop(0, pairs, query_step, 0)
 
     square = jnp.zeros((rows, 1), jnp.float32)
     for p in range(pairs):
@@ -400,6 +403,8 @@
         scratch_shapes=[
             pltpu.VMEM(kv_weight.shape, bf),
             pltpu.VMEM(gate.shape, bf),
+            pltpu.VMEM(latent.shape, bf),
+            pltpu.VMEM((ROPE, rows), bf),
             pltpu.VMEM((1, rank), jnp.float32),
             pltpu.VMEM(inner.shape, jnp.float32),
             pltpu.VMEM(outer.shape, jnp.float32),
@@ -412,10 +417,10 @@
             pltpu.VMEM((n_d, pairs, rows, PAIR), bf),
             pltpu.VMEM((heads, seq, KDIM), bf),
             pltpu.VMEM((heads, seq, 2 * VDIM), bf),
-            pltpu.VMEM((2 * rows, PAIR), bf),
+            pltpu.VMEM((n_d * rows, PAIR), bf),
             pltpu.VMEM((n_d, pairs, rows, 2 * VDIM), bf),
             pltpu.VMEM((n_d, pairs, rows, 2 * VDIM), bf),
-            dma, dma, dma((3,)),
+            dma, dma, dma((5,)),
             dma((n_z // 2, CHUNKS)), dma((n_z, CHUNKS)), dma((n_z // 2,)), dma((n_z,)),
             dma((n_z, half, CHUNKS)), dma((n_z, half)),
             *[dma((n_s,))] * 4,

time: 54.5 us -> 54.4 us (level)
  no operation moved by 1% of the time
where the time goes in v4:
time: 54.4 us; the launch traced here: 54.3 us
  Pallas kernels  52.9 us (97%)
  other arithmetic  1.25 us (2%)
    pallas_call x1, Pallas kernels, per_device(): pl.pallas_call(functools.partial(kernel, n_s, n_d), out_shape=(pltpu.VMEM...  52.9 us
    convert_element_type x1, other arithmetic, per_device(): return (gated * scale[:, :1] * out_gain[None, :]).astype(bf)  1.25 us

profile of v4, /device:TPU:1, one launch (start us, length us, event | category | flops | bytes accessed | tf_op | source)
XLA Modules:
  0.0 54.3 jit_solution(3098288213556095726)
XLA Ops:
  0.0 0.0 copy-start
  0.0 52.9 %latent_attention.1 = (f32[128,4096]{1,0:T(8,128)S(1)}, f32[128,128]{1,0:T(8,128)S(1)}) custom-call(bf16[128,6144]{1,0:T(8,128)(2,1)} %q_ref.1, bf16[128,1024]{1,0:T(8,128)(2,1)} %lat_hbm.1, bf16[64,128]{1,0:T(8,128)(2,1)} %bitcast.2, f32[1,1024]{1,0:T(1,128)} %bitcast.3, bf16[1024,2048]{1,0:T(8,128)(2,1)} %w_ref.1, bf16[128,4096]{1,0:T(8,128)(2,1)} %gate_ref.1, ...), custom_call_target="tpu_custom_call" | custom-call | tf_op jit(solution)/shard_map/latent_attention/pallas_call | solution.py:395
  52.9 0.1 slice_reduce_fusion
  53.0 0.0 copy-done
  53.0 1.3 %multiply_convert_fusion = bf16[128,4096]{1,0:T(8,128)(2,1)} fusion(f32[128,4096]{1,0:T(8,128)S(1)} %get-tuple-element.7, f32[4096]{0:T(1024)S(1)} %copy-done, f32[128]{0:T(128)S(1)} %slice_reduce_fusion), kind=kLoop, calls=%fused_computation | loop fusion | flops 1572864 | bytes 3162624 | tf_op jit(solution)/shard_map/convert_element_type | solution.py:436
Async XLA Ops:
  0.0 53.0 %copy-start = (f32[4096]{0:T(1024)S(1)}, f32[4096]{0:T(1024)}, u32[]{:S(2)}) copy-start(f32[4096]{0:T(1024)} %param.15) | copy-start | bytes 49156
